TPU v7x, 32 devices: a whole 2x2x4 slice. The times are simulated.
32 devices in a mesh: ep: 8 (over z, x), tp: 4 (over y, core).
Axes of the slice: x: 2, y: 2, z: 4, core: 2. Of those that a mesh axis runs over, the one named last changes fastest.
Arguments:
- mixer_input: bfloat16 [1024, 2048], P('ep'), may hold values from -6 to 6
- mixer_gain: float32 [2048], replicated, may hold values from 0.1 to 1.9
- outer_weight: bfloat16 [2048, 1024], P(None, 'tp'), may hold values from -0.125 to 0.125
- inner_weight: bfloat16 [2048, 1024], P(None, 'tp'), may hold values from -0.125 to 0.125
- value_weight: bfloat16 [2048, 1024], P(None, 'tp'), may hold values from -0.125 to 0.125
- conv_kernel: bfloat16 [3, 1024], P(None, 'tp'), may hold values from -3 to 3
- group_gain: float32 [1024], P('tp'), may hold values from 0.1 to 1.9
- mixer_out_weight: bfloat16 [1024, 2048], P(None, 'tp'), may hold values from -0.1875 to 0.1875
- expert_input: bfloat16 [2048, 2048], P('ep'), may hold values from -6 to 6
- expert_gain: float32 [2048], replicated, may hold values from 0.1 to 1.9
- routes: int32 [2048, 2], P('ep'), may hold values from 0 to 7, all different within a row; in each aligned block of 256 rows (0 to 255, 256 to 511, ...) at most 128 rows name the same one
- route_weight: float32 [2048, 2], P('ep'), may hold values from 0.1 to 1
- expert_gate: bfloat16 [8, 2048, 3584], P('ep', None, 'tp'), may hold values from -0.125 to 0.125
- expert_up: bfloat16 [8, 2048, 3584], P('ep', None, 'tp'), may hold values from -0.125 to 0.125
- expert_down: bfloat16 [8, 3584, 2048], P('ep', None, 'tp'), may hold values from -0.09375 to 0.09375
Outputs:
- mixed_tokens: bfloat16 [1024, 2048], P('ep', 'tp')
- expert_tokens: bfloat16 [2048, 2048], P('ep', 'tp')
Inputs may be any that keep to these rules, and one draw needn't show every extreme that they name: `routes`: each row names 2 different experts. Within the rows of one index of ep no expert is named by more than 128 rows, a bound that some block reaches of them.
All inputs are finite; a program needn't handle non-finite values.
Results may differ from a plain program's by a relative error of at most 0.014.
Values may be sent and summed in bfloat16 or wider, within the bound.
A program may use at most 64 MiB of HBM per device.

v0:
```python
import jax
import jax.numpy as jnp
from jax import lax
from jax.sharding import PartitionSpec as P

GROUP = 64


EPS = 1e-06


def from_behind(block, axis, distance):
    devices = range(lax.axis_size(axis))
    route = [(i - distance, i) for i in devices if i - distance in devices]
    return lax.ppermute(block, axis, route)


def rms_scale(values, gain):
    floats = values.astype(jnp.float32)
    scale = lax.rsqrt(jnp.mean(floats * floats, axis=-1, keepdims=True) + EPS)
    return floats * scale * gain


def per_device(
    mixer_input,
    mixer_gain,
    outer_weight,
    inner_weight,
    value_weight,
    conv_kernel,
    group_gain,
    mixer_out_weight,
    expert_input,
    expert_gain,
    routes,
    route_weight,
    expert_gate,
    expert_up,
    expert_down,
):
    mix_count = mixer_input.shape[0]
    normed_a = rms_scale(mixer_input, mixer_gain).astype(jnp.bfloat16)
    outer = jnp.dot(normed_a, outer_weight, preferred_element_type=jnp.float32).astype(jnp.bfloat16)
    inner = jnp.dot(normed_a, inner_weight, preferred_element_type=jnp.float32).astype(jnp.bfloat16)
    values = jnp.dot(normed_a, value_weight, preferred_element_type=jnp.float32).astype(
        jnp.bfloat16
    )
    product = inner.astype(jnp.float32) * values.astype(jnp.float32)
    earlier_rows = from_behind(product[mix_count - 2 :], "ep", 1)
    padded = jnp.concatenate([earlier_rows, product], axis=0)
    kernel = conv_kernel.astype(jnp.float32)
    conv_sum = (
        kernel[0] * padded[0:mix_count]
        + kernel[1] * padded[1 : mix_count + 1]
        + kernel[2] * padded[2 : mix_count + 2]
    )
    gated = outer.astype(jnp.float32) * conv_sum
    grouped = gated.reshape(mix_count, -1, GROUP)
    grouped = rms_scale(grouped, group_gain.reshape(-1, GROUP))
    grouped = grouped.reshape(mix_count, -1).astype(jnp.bfloat16)
    weight_rows = mixer_out_weight
    mixed_tokens = jnp.dot(
        lax.all_gather(grouped, "tp", axis=1, tiled=True),
        weight_rows,
        preferred_element_type=jnp.float32,
    ).astype(jnp.bfloat16)
    exp_count, picks_each = routes.shape
    width = expert_input.shape[1]
    experts = expert_gate.shape[0] * lax.axis_size("ep")
    capacity = 2 * picks_each * exp_count // experts
    normed_b = rms_scale(expert_input, expert_gain).astype(jnp.bfloat16)
    picks = routes.reshape(-1)
    onehot = (picks[:, None] == jnp.arange(experts, dtype=jnp.int32)[None, :]).astype(jnp.int32)
    rank = jnp.sum((jnp.cumsum(onehot, axis=0) - onehot) * onehot, axis=1)
    slot = picks * capacity + rank
    token = jnp.arange(exp_count * picks_each, dtype=jnp.int32) // picks_each
    table = jnp.zeros((experts * capacity,), jnp.int32).at[slot].set(token + 1)
    valid = table > 0
    gathered_rows = jnp.take(normed_b, jnp.maximum(table - 1, 0), axis=0)
    buffer = jnp.where(valid[:, None], gathered_rows, 0).reshape(experts, capacity, width)
    gate_weight = expert_gate[0]
    up_weight = expert_up[0]
    down_weight = expert_down[0]
    out_cols = down_weight.shape[1]
    span = width // lax.axis_size("tp")
    outgoing = lax.dynamic_slice_in_dim(buffer, lax.axis_index("tp") * span, span, 2)
    received = lax.all_to_all(outgoing, "ep", split_axis=0, concat_axis=0, tiled=True)
    sources = received.shape[0]
    count = received.shape[1]
    piece = lax.all_gather(received, "tp", axis=2, tiled=True)
    span = piece.shape[2]
    flat_piece = piece.reshape(sources * count, span)
    gate = jnp.dot(flat_piece, gate_weight, preferred_element_type=jnp.float32)
    up_value = jnp.dot(flat_piece, up_weight, preferred_element_type=jnp.float32)
    hidden = (jax.nn.silu(gate) * up_value).astype(jnp.bfloat16)
    weight_rows = down_weight
    results = jnp.dot(
        lax.all_gather(hidden, "tp", axis=1, tiled=True),
        weight_rows,
        preferred_element_type=jnp.float32,
    ).astype(jnp.bfloat16)
    returned = lax.all_to_all(
        results.reshape(sources, count, out_cols), "ep", split_axis=0, concat_axis=0, tiled=True
    )
    flat_returned = returned.reshape(experts * capacity, out_cols)
    chosen = (
        jnp.take(flat_returned, slot, axis=0)
        .astype(jnp.float32)
        .reshape(exp_count, picks_each, out_cols)
    )
    weighted = jnp.sum(chosen * route_weight[..., None], axis=1)
    expert_tokens = weighted.astype(jnp.bfloat16)
    return (mixed_tokens, expert_tokens)


def solution(mesh):
    placed = (
        P("ep", None),
        P(),
        P(None, "tp"),
        P(None, "tp"),
        P(None, "tp"),
        P(None, "tp"),
        P("tp"),
        P(None, "tp"),
        P("ep", None),
        P(),
        P("ep", None),
        P("ep", None),
        P("ep", None, "tp"),
        P("ep", None, "tp"),
        P("ep", None, "tp"),
    )
    return jax.shard_map(
        per_device,
        mesh=mesh,
        in_specs=placed,
        out_specs=(P("ep", "tp"), P("ep", "tp")),
        check_vma=False,
    )
```

profile of v0, /device:TPU:17, one launch (start us, length us, event | category | flops | bytes accessed | tf_op | source)
XLA Modules:
  0.0 217.8 jit_solution(1742705976058529025)
XLA Ops:
  7.2 0.9 copy.27
  8.1 0.1 eq.26
  8.4 0.7 broadcast_multiply_fusion
  9.1 1.1 reduce-window.6
  10.3 0.2 slice_reduce_fusion
  10.7 0.1 mul.166
  10.9 2.4 %scatter_custom_fusion = s32[1024]{0:T(1024)S(1)} fusion(s32[512]{0:T(512)S(1)} %bitcast.50, s32[512]{0:T(512)S(1)} %fusion.32, s32[]{:T(128)} %constant.74.clone.1), kind=kCustom, calls=%fused_computation.66 | custom fusion | bytes 4100 | tf_op jit(solution)/shard_map/scatter | solution.py:77
  13.4 1.5 fusion.8
  14.9 1.5 fusion.10
  16.5 6.0 %gather_fusion = bf16[1024,2048]{1,0:T(8,128)(2,1)} fusion(bf16[256,2048]{1,0:T(8,128)(2,1)S(1)} %fusion.10, s32[1024]{0:T(1024)S(1)} %fusion.31), kind=kCustom, calls=%fused_computation | custom fusion | bytes 8392704 | tf_op jit(solution)/shard_map/jit(_take)/gather | solution.py:79
  22.5 1.5 fusion.21
  24.0 29.2 %all_to_all.10 = bf16[8,128,512]{2,1,0:T(8,128)(2,1)} all-to-all(bf16[8,128,512]{2,1,0:T(8,128)(2,1)S(1)} %fusion.21), channel_id=1, replica_groups=mesh['ep'=8,'tp'=4] {'ep'}, dimensions={0} | all-to-all | bytes 2097152 | tf_op jit(solution)/shard_map/all_to_all | solution.py:87
  53.2 36.1 %all-gather.3.cloned.1.call-done = bf16[8,128,2048]{2,1,0:T(8,128)(2,1)} async-done(((bf16[8,128,512]{2,1,0:T(8,128)(2,1)}), bf16[8,128,2048]{2,1,0:T(8,128)(2,1)}) %all-gather.3.cloned.1.call-update) | async-done | bytes 4194320 | tf_op jit(solution)/shard_map/all_gather | solution.py:90
  89.4 7.5 %fusion.2 = f32[1024,896]{1,0:T(8,128)S(1)} fusion(bf16[1024,2048]{1,0:T(8,128)(2,1)} %bitcast.55, bf16[1,2048,896]{2,1,0:T(8,128)(2,1)} %param.28), kind=kOutput, calls=%fused_computation.5 | convolution fusion | flops 3758096384 | bytes 11534336 | tf_op jit(solution)/shard_map/dot_general | solution.py:94
  96.9 6.0 %multiply_convert_fusion = bf16[1024,896]{1,0:T(8,128)(2,1)} fusion(f32[1024,896]{1,0:T(8,128)S(1)} %fusion.2, bf16[1024,2048]{1,0:T(8,128)(2,1)S(1)} %bitcast.56, bf16[1,2048,896]{2,1,0:T(8,128)(2,1)S(1)} %copy-done.10), kind=kOutput, calls=%fused_computation.9 | convolution fusion | flops 3763601408 | bytes 13369344 | tf_op jit(solution)/shard_map/dot_general | solution.py:93
  103.0 0.2 fusion.18
  103.2 0.4 fusion.16
  103.6 51.8 %all-gather.5.cloned.1.call-done = bf16[1024,3584]{1,0:T(8,128)(2,1)} async-done(((bf16[1024,896]{1,0:T(8,128)(2,1)}), bf16[1024,3584]{1,0:T(8,128)(2,1)}) %all-gather.5.cloned.1.call-update) | async-done | bytes 7340048 | tf_op jit(solution)/shard_map/all_gather | solution.py:98
  155.4 9.0 %fusion.11 = bf16[1024,512]{1,0:T(8,128)(2,1)} fusion(bf16[1024,3584]{1,0:T(8,128)(2,1)} %all-gather.5.cloned.1.call-done, bf16[1,3584,512]{2,1,0:T(8,128)(2,1)} %param.29), kind=kOutput, calls=%fused_computation.15 | convolution fusion | flops 3758620672 | bytes 12058624 | tf_op jit(solution)/shard_map/dot_general | solution.py:97
  164.5 5.6 %all-to-all-start.1 = ((bf16[8,128,512]{2,1,0:T(8,128)(2,1)}), bf16[8,128,512]{2,1,0:T(8,128)(2,1)S(1)}, u32[]{:S(2)}, u32[]{:S(2)}) async-start(bf16[8,128,512]{2,1,0:T(8,128)(2,1)} %bitcast.47), calls=%async_computation.1 | async-start | bytes 2097152 | tf_op jit(solution)/shard_map/all_to_all | solution.py:102
  170.1 1.7 fusion.15
  171.9 0.6 copy-done.8
  172.5 3.1 %collective-permute-start = (f32[2,256]{1,0:T(2,128)S(1)}, f32[2,256]{1,0:T(2,128)S(1)}, u32[]{:S(2)}, u32[]{:S(2)}) collective-permute-start(f32[2,256]{1,0:T(2,128)S(1)} %slice.37), channel_id=1, source_target_pairs={{0,4},{4,8},{8,12},{12,16},{16,20},{20,24},{24,28},{1,5},{5,9},{9,... | collective-permute-start | bytes 6152 | tf_op jit(solution)/shard_map/ppermute | solution.py:15
  175.9 0.8 copy.30
  176.8 18.1 %collective-permute-done = f32[2,256]{1,0:T(2,128)S(1)} collective-permute-done((f32[2,256]{1,0:T(2,128)S(1)}, f32[2,256]{1,0:T(2,128)S(1)}, u32[]{:S(2)}, u32[]{:S(2)}) %collective-permute-start) | collective-permute-done | bytes 2080 | tf_op jit(solution)/shard_map/ppermute | solution.py:15
  194.9 2.2 fusion.44
  197.3 0.9 multiply_convert_fusion.1
  198.2 6.6 %all_gather.9 = bf16[128,1024]{1,0:T(8,128)(2,1)S(1)} all-gather(bf16[128,256]{1,0:T(8,128)(2,1)S(1)} %multiply_convert_fusion.1), channel_id=1, replica_groups=mesh['ep'=8,'tp'=4] {'tp'}, dimensions={1}, use_global_device_ids=true | all-gather | bytes 327680 | tf_op jit(solution)/shard_map/all_gather | solution.py:63
  204.8 1.0 convolution_convert_fusion
  205.8 2.0 gather_fusion.1
  207.8 0.2 gather.15
  208.0 2.9 %multiply_reduce_fusion = bf16[256,512]{1,0:T(8,128)(2,1)} fusion(bf16[256,2,512]{2,1,0:T(2,128)(2,1)S(1)} %gather.15, pred[256,2]{1,0:T(8,128)(4,1)S(1)} %copy-done.3, f32[256,2]{1,0:T(8,128)S(1)} %copy.32), kind=kLoop, calls=%fused_computation.31 | loop fusion | flops 917504 | bytes 788992 | tf_op jit(solution)/shard_map/reduce_sum | solution.py:111
  (54 shorter events, 1.2 us)
Async XLA Ops:
  7.2 187.7 %copy-start = (bf16[2048,256]{1,0:T(8,128)(2,1)S(1)}, bf16[2048,256]{1,0:T(8,128)(2,1)}, u32[]{:S(2)}) copy-start(bf16[2048,256]{1,0:T(8,128)(2,1)} %param.17) | copy-start | bytes 3145732
  7.2 82.2 %all-gather.3.cloned.1.call-start = ((), (), s32[]{:S(2)}) async-start(), calls=%async_computation.2 | async-start | bytes 5242880 | tf_op jit(solution)/shard_map/all_gather | solution.py:90
  53.2 102.2 %all-gather.5.cloned.1.call-start = ((), (), s32[]{:S(2)}) async-start(), calls=%async_computation.3 | async-start | bytes 9175040 | tf_op jit(solution)/shard_map/all_gather | solution.py:98
  89.4 7.5 %copy-start.9 = (bf16[8,128,2048]{2,1,0:T(8,128)(2,1)S(1)}, bf16[8,128,2048]{2,1,0:T(8,128)(2,1)}, u32[]{:S(2)}) copy-start(bf16[8,128,2048]{2,1,0:T(8,128)(2,1)} %all-gather.3.cloned.1.call-done) | copy-start | bytes 12582916
  89.4 7.5 %copy-start.10 = (bf16[1,2048,896]{2,1,0:T(8,128)(2,1)S(1)}, bf16[1,2048,896]{2,1,0:T(8,128)(2,1)}, u32[]{:S(2)}) copy-start(bf16[1,2048,896]{2,1,0:T(8,128)(2,1)} %param.27) | copy-start | bytes 11010052
  96.9 6.1 %copy-start.2 = (bf16[128,2048]{1,0:T(8,128)(2,1)S(1)}, bf16[128,2048]{1,0:T(8,128)(2,1)}, u32[]{:S(2)}) copy-start(bf16[128,2048]{1,0:T(8,128)(2,1)} %param.15) | copy-start | bytes 1572868
  96.9 6.3 %copy-start.11 = (bf16[2048,256]{1,0:T(8,128)(2,1)S(1)}, bf16[2048,256]{1,0:T(8,128)(2,1)}, u32[]{:S(2)}) copy-start(bf16[2048,256]{1,0:T(8,128)(2,1)} %param.18) | copy-start | bytes 3145732
  96.9 6.3 %copy-start.12 = (f32[2048]{0:T(1024)S(1)}, f32[2048]{0:T(1024)}, u32[]{:S(2)}) copy-start(f32[2048]{0:T(1024)} %param.16) | copy-start | bytes 24580
  164.4 11.4 %copy-start.4 = (s32[256,2]{0,1:T(2,128)S(1)}, s32[256,2]{0,1:T(2,128)}, u32[]{:S(2)}) copy-start(s32[256,2]{0,1:T(2,128)} %param.25) | copy-start | bytes 6148
  164.5 11.4 %copy-start.5 = (bf16[3,256]{1,0:T(4,128)(2,1)S(1)}, bf16[3,256]{1,0:T(4,128)(2,1)}, u32[]{:S(2)}) copy-start(bf16[3,256]{1,0:T(4,128)(2,1)} %param.20) | copy-start | bytes 4612
  164.5 12.2 %copy-start.6 = (f32[256,2]{0,1:T(2,128)S(1)}, f32[256,2]{0,1:T(2,128)}, u32[]{:S(2)}) copy-start(f32[256,2]{0,1:T(2,128)} %param.26) | copy-start | bytes 6148
  164.5 32.8 %copy-start.7 = (f32[256]{0:T(256)S(1)}, f32[256]{0:T(256)}, u32[]{:S(2)}) copy-start(f32[256]{0:T(256)} %param.21) | copy-start | bytes 3076
  164.5 40.4 %copy-start.1 = (bf16[1024,512]{1,0:T(8,128)(2,1)S(1)}, bf16[1024,512]{1,0:T(8,128)(2,1)}, u32[]{:S(2)}) copy-start(bf16[1024,512]{1,0:T(8,128)(2,1)} %param.22) | copy-start | bytes 3145732
  164.5 41.3 %all-to-all-start.1 = ((bf16[8,128,512]{2,1,0:T(8,128)(2,1)}), bf16[8,128,512]{2,1,0:T(8,128)(2,1)S(1)}, u32[]{:S(2)}, u32[]{:S(2)}) async-start(bf16[8,128,512]{2,1,0:T(8,128)(2,1)} %bitcast.47), calls=%async_computation.1 | async-start | bytes 2097152 | tf_op jit(solution)/shard_map/all_to_all | solution.py:102
  171.8 0.7 copy-start.8
  172.5 22.4 %collective-permute-start = (f32[2,256]{1,0:T(2,128)S(1)}, f32[2,256]{1,0:T(2,128)S(1)}, u32[]{:S(2)}, u32[]{:S(2)}) collective-permute-start(f32[2,256]{1,0:T(2,128)S(1)} %slice.37), channel_id=1, source_target_pairs={{0,4},{4,8},{8,12},{12,16},{16,20},{20,24},{24,28},{1,5},{5,9},{9,... | collective-permute-start | bytes 6152 | tf_op jit(solution)/shard_map/ppermute | solution.py:15
  204.8 3.2 %copy-start.3 = (pred[256,2]{1,0:T(8,128)(4,1)S(1)}, pred[256,2]{1,0:T(8,128)(4,1)}, u32[]{:S(2)}) copy-start(pred[256,2]{1,0:T(8,128)(4,1)} %copy.30) | copy-start | bytes 1540
Sparse Core Ops, SparseCore 0:
  53.3 35.9 all-gather.2
  103.1 52.2 all-gather.4
where the time goes:
time: 218 us
  waiting for transfers between devices  106 us (49%)
  blocking collectives  35.8 us (16%)
  matrix products  27.8 us (13%)
  between operations  14.4 us (7%)
  local copies, waits for them, and re-layouts  14.3 us (7%)
  other arithmetic  10.6 us (5%)
  starting transfers between devices  8.77 us (4%)
    all_gather x1, waiting for transfers between devices, per_device(): lax.all_gather(hidden, 'tp', axis=1, tiled=True)  51.8 us
    all_gather x1, waiting for transfers between devices, per_device(): piece = lax.all_gather(received, 'tp', axis=2, tiled=True)  36.1 us
    all_to_all x1, blocking collectives, per_device(): lax.all_to_all(outgoing, 'ep', split_axis=0, concat_axis=0, tiled=True)  29.2 us
    ppermute x1, waiting for transfers between devices, from_behind(): return lax.ppermute(block, axis, route)  18.1 us
    dot_general x1, matrix products, per_device(): jnp.dot(lax.all_gather(hidden, 'tp', axis=1, tiled=True), weight_rows, pr...  9.04 us
    dot_general x1, matrix products, per_device(): jnp.dot(flat_piece, up_weight, preferred_element_type=jnp.float32)  7.49 us
    all_gather x1, blocking collectives, per_device(): lax.all_gather(grouped, 'tp', axis=1, tiled=True)  6.58 us
    dot_general x1, matrix products, per_device(): gate = jnp.dot(flat_piece, gate_weight, preferred_element_type=jnp.float32)  6.04 us
  transfers between devices with their start and end apart: 4, of which 3 were waited for; matrix products, arithmetic and copies ran while one was open for 4% of the time, Pallas kernels for 0%

commit v1 on v0

--- a/solution.py
+++ b/solution.py
@@ -1,6 +1,10 @@
+import functools
+
 import jax
 import jax.numpy as jnp
 from jax import lax
+from jax.experimental import pallas as pl
+from jax.experimental.pallas import tpu as pltpu
 from jax.sharding import PartitionSpec as P
 
 GROUP = 64
@@ -21,7 +25,339 @@
     return floats * scale * gain
 
 
-def per_device(
+F32 = jnp.float32
+BF16 = jnp.bfloat16
+
+
+def flip(index, offset, count):
+    out = index
+    bit = 1
+    while bit < count:
+        if offset & bit:
+            out = out + bit - 2 * bit * ((index // bit) % 2)
+        bit *= 2
+    return out
+
+
+def matmul(a, b):
+    return jnp.dot(a, b, preferred_element_type=F32)
+
+
+def experts_kernel(
+    n_ep,
+    x_ref,
+    gain_ref,
+    routes_ref,
+    weight_ref,
+    gate_hbm,
+    up_hbm,
+    down_hbm,
+    o_ref,
+    nb,
+    xs,
+    xb,
+    wgu,
+    wd,
+    hb,
+    rs,
+    ret,
+    whi,
+    wlo,
+    w_sem,
+    s_sem,
+    r_sem,
+):
+    ep = lax.axis_index("ep")
+    tp = lax.axis_index("tp")
+    y, core = tp // 2, tp % 2
+    partner = {"tp": y * 2 + 1 - core}
+    across = {"tp": (1 - y) * 2 + core}
+    over_tp = (1 - y) * 2 + core
+    half = n_ep // 2
+    rows = x_ref.shape[0]
+    cap = xb.shape[2]
+    span = xb.shape[3]
+    tiles, depth, pair = wgu.shape
+    tile = pair // 2
+    part = hb.shape[3]
+    out_cols = wd.shape[1]
+
+    barrier = pltpu.get_barrier_semaphore()
+    peers = [{"ep": flip(ep, m, n_ep)} for m in range(1, n_ep)] + [partner, across]
+    for peer in peers:
+        pl.semaphore_signal(barrier, inc=1, device_id=peer, device_id_type=pl.DeviceIdType.MESH)
+
+    fetches = []
+    for j in range(tiles):
+        cols = pl.ds(j * tile, tile)
+        fetches.append(
+            (
+                pltpu.make_async_copy(
+                    gate_hbm.at[0, :, cols], wgu.at[j, :, pl.ds(0, tile)], w_sem.at[2 * j]
+                ),
+                pltpu.make_async_copy(
+                    up_hbm.at[0, :, cols], wgu.at[j, :, pl.ds(tile, tile)], w_sem.at[2 * j + 1]
+                ),
+            )
+        )
+    fetch_down = pltpu.make_async_copy(down_hbm.at[0], wd, w_sem.at[2 * tiles])
+    for a, b in fetches:
+        a.start()
+        b.start()
+    fetch_down.start()
+
+    step_rows = 32
+
+    def norm(i, carry):
+        at = pl.ds(pl.multiple_of(i * step_rows, step_rows), step_rows)
+        v = x_ref[at, :].astype(F32)
+        scale = lax.rsqrt(jnp.mean(v * v, axis=-1, keepdims=True) + EPS)
+        nb[at, :] = (v * scale * gain_ref[...]).astype(BF16)
+        return carry
+
+    lax.fori_loop(0, rows // step_rows, norm, 0)
+
+    first = routes_ref[0:1, :]
+    second = routes_ref[1:2, :]
+    masks = []
+    level = lax.broadcasted_iota(jnp.int32, (n_ep, rows), 0)
+    stacked = jnp.zeros((n_ep, rows), F32)
+    for m in range(n_ep):
+        e = flip(ep, m, n_ep)
+        mask = jnp.where((first == e) | (second == e), 1.0, 0.0)
+        masks.append(mask)
+        stacked = jnp.where(level == m, mask, stacked)
+    upper = lax.broadcasted_iota(jnp.int32, (rows, rows), 0) < lax.broadcasted_iota(
+        jnp.int32, (rows, rows), 1
+    )
+    ranks = matmul(stacked.astype(BF16), jnp.where(upper, 1.0, 0.0).astype(BF16))
+    slots = lax.broadcasted_iota(jnp.int32, (cap, rows), 0).astype(F32)
+    place = []
+    for m in range(n_ep):
+        place.append(jnp.where((slots == ranks[m : m + 1, :]) & (masks[m] > 0.5), 1.0, 0.0))
+
+    def remote(src, dst, kind, m, device):
+        return pltpu.make_async_remote_copy(
+            src_ref=src,
+            dst_ref=dst,
+            send_sem=s_sem.at[kind, m],
+            recv_sem=r_sem.at[kind, m],
+            device_id=device,
+            device_id_type=pl.DeviceIdType.MESH,
+        )
+
+    mine2 = pl.ds(core * 2, 2)
+    from_source, to_partner, to_across, relay = [None] * n_ep, {}, {}, {}
+    for m in range(1, n_ep):
+        peer = {"ep": flip(ep, m, n_ep)}
+        if m < half:
+            from_source[m] = remote(xs.at[m], xb.at[m, mine2], 0, m, peer)
+            to_partner[m] = remote(xb.at[m, mine2], xb.at[m, mine2], 1, m, partner)
+        else:
+            from_source[m] = remote(xs.at[m, 0], xb.at[m, tp], 0, m, peer)
+            to_partner[m] = remote(xb.at[m, tp], xb.at[m, tp], 1, m, partner)
+            to_across[m] = remote(xb.at[m, tp], xb.at[m, tp], 2, m, across)
+            relay[m] = remote(xb.at[m, over_tp], xb.at[m, over_tp], 3, m, partner)
+    hid_partner, hid_across, hid_relay, back = [], [], [], [None] * n_ep
+    for m in range(n_ep):
+        hid_partner.append(remote(hb.at[m, tp], hb.at[m, tp], 4, m, partner))
+        hid_across.append(remote(hb.at[m, tp], hb.at[m, tp], 5, m, across))
+        hid_relay.append(remote(hb.at[m, over_tp], hb.at[m, over_tp], 6, m, partner))
+        if m:
+            back[m] = remote(rs.at[m], ret.at[m], 7, m, {"ep": flip(ep, m, n_ep)})
+
+    for m in range(1, n_ep):
+        chosen = place[m].astype(BF16)
+        if m < half:
+            for k in range(2):
+                at = pl.ds(pl.multiple_of((core * 2 + k) * span, span), span)
+                xs[m, k] = matmul(chosen, nb[:, at]).astype(BF16)
+        else:
+            at = pl.ds(pl.multiple_of(tp * span, span), span)
+            xs[m, 0] = matmul(chosen, nb[:, at]).astype(BF16)
+        if m == 1:
+            pl.semaphore_wait(barrier, len(peers))
+        from_source[m].start()
+    chosen = place[0].astype(BF16)
+    for k in range(depth // span):
+        xb[0, k] = matmul(chosen, nb[:, k * span : (k + 1) * span]).astype(BF16)
+
+    def expand(m):
+        def body(j, carry):
+            if m == 0:
+                pltpu.make_async_copy(
+                    gate_hbm.at[0, :, pl.ds(0, tile)], wgu.at[j, :, pl.ds(0, tile)], w_sem.at[2 * j]
+                ).wait()
+                pltpu.make_async_copy(
+                    up_hbm.at[0, :, pl.ds(0, tile)],
+                    wgu.at[j, :, pl.ds(tile, tile)],
+                    w_sem.at[2 * j + 1],
+                ).wait()
+            acc = matmul(xb[m, 0], wgu[j, 0:span, :])
+            for k in range(1, depth // span):
+                acc = acc + matmul(xb[m, k], wgu[j, k * span : (k + 1) * span, :])
+            g, u = acc[:, :tile], acc[:, tile:]
+            hidden = g / (1.0 + jnp.exp(-g)) * u
+            hb[m, tp, :, pl.ds(pl.multiple_of(j * tile, tile), tile)] = hidden.astype(BF16)
+            return carry
+
+        lax.fori_loop(0, tiles, body, 0)
+        hid_across[m].start()
+        hid_partner[m].start()
+
+    block = 256
+
+    def contract(m):
+        hid_partner[m].wait_recv()
+        hid_relay[m].wait_recv()
+        for n in range(out_cols // block):
+            cols = slice(n * block, (n + 1) * block)
+            acc = matmul(hb[m, 0], wd[0:part, cols])
+            for k in range(1, hb.shape[1]):
+                acc = acc + matmul(hb[m, k], wd[k * part : (k + 1) * part, cols])
+            if m == 0:
+                ret[0, :, cols] = acc.astype(BF16)
+            else:
+                rs[m, :, cols] = acc.astype(BF16)
+        if m:
+            back[m].start()
+
+    def pass_hidden(m):
+        hid_across[m].wait_recv()
+        hid_relay[m].start()
+
+    def pass_near(m):
+        from_source[m].wait_recv()
+        to_partner[m].start()
+
+    def pass_far(m):
+        from_source[m].wait_recv()
+        to_across[m].start()
+        to_partner[m].start()
+
+    def pass_relay(m):
+        to_across[m].wait_recv()
+        relay[m].start()
+
+    def ready(m):
+        to_partner[m].wait_recv()
+        if m >= half:
+            relay[m].wait_recv()
+
+    expand(0)
+    for m in range(n_ep):
+        picked = jnp.where(first == flip(ep, m, n_ep), weight_ref[0:1, :], weight_ref[1:2, :])
+        scaled = (place[m] * picked).T
+        high = scaled.astype(BF16)
+        whi[:, m * cap : (m + 1) * cap] = high
+        wlo[:, m * cap : (m + 1) * cap] = (scaled - high.astype(F32)).astype(BF16)
+    for m in range(1, half):
+        pass_near(m)
+        ready(m)
+        expand(m)
+        if m == 1:
+            fetch_down.wait()
+        if m >= 2:
+            pass_hidden(m - 2)
+            contract(m - 2)
+    for m in range(half, n_ep):
+        pass_far(m)
+        if m == half:
+            pass_hidden(half - 2)
+            contract(half - 2)
+    pass_hidden(half - 1)
+    for m in range(half, n_ep):
+        pass_relay(m)
+        ready(m)
+        expand(m)
+        if m == half:
+            contract(half - 1)
+        if m - 2 >= half:
+            pass_hidden(m - 2)
+            contract(m - 2)
+    pass_hidden(n_ep - 2)
+    contract(n_ep - 2)
+    pass_hidden(n_ep - 1)
+    contract(n_ep - 1)
+
+    total = None
+    for m in range(n_ep):
+        if m:
+            back[m].wait_recv()
+        high = matmul(whi[:, m * cap : (m + 1) * cap], ret[m])
+        low = matmul(wlo[:, m * cap : (m + 1) * cap], ret[m])
+        total = high + low if total is None else total + (high + low)
+    o_ref[...] = total.astype(BF16)
+
+    for m in range(n_ep):
+        for copy in (hid_partner[m], hid_across[m], hid_relay[m], from_source[m], back[m]):
+            if copy is not None:
+                copy.wait_send()
+        for table in (to_partner, to_across, relay):
+            if m in table:
+                table[m].wait_send()
+
+
+def experts_fused(
+    expert_input, expert_gain, routes, route_weight, expert_gate, expert_up, expert_down
+):
+    n_ep, n_tp = lax.axis_size("ep"), lax.axis_size("tp")
+    rows, width = expert_input.shape
+    cap = 2 * routes.shape[1] * rows // n_ep
+    span = width // n_tp
+    part = expert_gate.shape[2]
+    tile = 128
+    tiles = part // tile
+    full, out_cols = expert_down.shape[1:]
+    vmem = pl.BlockSpec(memory_space=pltpu.VMEM)
+    hbm = pl.BlockSpec(memory_space=pl.ANY)
+    return pl.pallas_call(
+        functools.partial(experts_kernel, n_ep),
+        out_shape=jax.ShapeDtypeStruct((rows, out_cols), BF16),
+        in_specs=[vmem] * 4 + [hbm] * 3,
+        out_specs=vmem,
+        scratch_shapes=[
+            pltpu.VMEM((rows, width), BF16),
+            pltpu.VMEM((n_ep, 2, cap, span), BF16),
+            pltpu.VMEM((n_ep, n_tp, cap, span), BF16),
+            pltpu.VMEM((tiles, width, 2 * tile), BF16),
+            pltpu.VMEM((full, out_cols), BF16),
+            pltpu.VMEM((n_ep, n_tp, cap, part), BF16),
+            pltpu.VMEM((n_ep, cap, out_cols), BF16),
+            pltpu.VMEM((n_ep, cap, out_cols), BF16),
+            pltpu.VMEM((rows, n_ep * cap), BF16),
+            pltpu.VMEM((rows, n_ep * cap), BF16),
+            pltpu.SemaphoreType.DMA((2 * tiles + 1,)),
+            pltpu.SemaphoreType.DMA((8, n_ep)),
+            pltpu.SemaphoreType.DMA((8, n_ep)),
+        ],
+        compiler_params=pltpu.CompilerParams(
+            collective_id=0, has_side_effects=True, vmem_limit_bytes=56 * 1024 * 1024
+        ),
+        name="experts",
+    )(
+        expert_input,
+        expert_gain.reshape(1, -1),
+        routes.T,
+        route_weight.T,
+        expert_gate,
+        expert_up,
+        expert_down,
+    )
+
+
+def fits(n_ep, n_tp, routes, expert_gate):
+    return (
+        n_tp == 4
+        and n_ep >= 4
+        and n_ep & (n_ep - 1) == 0
+        and routes.shape[1] == 2
+        and expert_gate.shape[0] == 1
+        and expert_gate.shape[2] % 128 == 0
+    )
+
+
+def mixer_xla(
     mixer_input,
     mixer_gain,
     outer_weight,
@@ -30,13 +366,6 @@
     conv_kernel,
     group_gain,
     mixer_out_weight,
-    expert_input,
-    expert_gain,
-    routes,
-    route_weight,
-    expert_gate,
-    expert_up,
-    expert_down,
 ):
     mix_count = mixer_input.shape[0]
     normed_a = rms_scale(mixer_input, mixer_gain).astype(jnp.bfloat16)
@@ -64,6 +393,18 @@
         weight_rows,
         preferred_element_type=jnp.float32,
     ).astype(jnp.bfloat16)
+    return mixed_tokens
+
+
+def experts_xla(
+    expert_input,
+    expert_gain,
+    routes,
+    route_weight,
+    expert_gate,
+    expert_up,
+    expert_down,
+):
     exp_count, picks_each = routes.shape
     width = expert_input.shape[1]
     experts = expert_gate.shape[0] * lax.axis_size("ep")
@@ -110,7 +451,15 @@
     )
     weighted = jnp.sum(chosen * route_weight[..., None], axis=1)
     expert_tokens = weighted.astype(jnp.bfloat16)
-    return (mixed_tokens, expert_tokens)
+    return expert_tokens
+
+
+def per_device(*args):
+    mixed = mixer_xla(*args[:8])
+    n_ep, n_tp = lax.axis_size("ep"), lax.axis_size("tp")
+    if fits(n_ep, n_tp, args[10], args[12]):
+        return mixed, experts_fused(*args[8:])
+    return mixed, experts_xla(*args[8:])
 
 
 def solution(mesh):

time: 218 us -> 95.9 us (0.44)
  the two profiles are of different devices: /device:TPU:17 before, /device:TPU:18 now
where the time goes in v1:
time: 95.9 us; the launch traced here: 94.4 us
  Pallas kernels  77.1 us (80%)
  blocking collectives  5.78 us (6%)
  matrix products  4.84 us (5%)
  starting transfers between devices  3.45 us (4%)
  other arithmetic  1.38 us (1%)
    pallas_call x1, Pallas kernels, experts_fused(): pl.pallas_call(functools.partial(experts_kernel, n_ep), out_shape=jax.Sha...  77.1 us
    all_gather x1, blocking collectives, mixer_xla(): lax.all_gather(grouped, 'tp', axis=1, tiled=True)  5.78 us
    ppermute x1, starting transfers between devices, from_behind(): return lax.ppermute(block, axis, route)  3.45 us
  transfers between devices with their start and end apart: 1, of which 0 were waited for; matrix products, arithmetic and copies ran while one was open for 0% of the time, Pallas kernels for 82%

profile of v1, /device:TPU:18, one launch (start us, length us, event | category | flops | bytes accessed | tf_op | source)
XLA Modules:
  0.0 94.4 jit_solution(14077808356050826845)
XLA Ops:
  0.6 0.0 copy-start
  0.6 0.0 copy-start.4
  0.7 1.3 %fusion.4 = f32[128]{0:T(128)S(1)} fusion(bf16[128,2048]{1,0:T(8,128)(2,1)} %param.15), kind=kLoop, calls=%fused_computation.10 | loop fusion | flops 786304 | bytes 524800 | tf_op jit(solution)/shard_map/reduce_sum | solution.py:24
  2.0 1.8 %fusion.2 = f32[128,256]{1,0:T(8,128)S(1)} fusion(bf16[2048,256]{1,0:T(8,128)(2,1)} %param.18, bf16[128,2048]{1,0:T(8,128)(2,1)} %param.15, f32[2048]{0:T(1024)} %param.16, f32[128]{0:T(128)S(1)} %add_rsqrt_fusion.1), kind=kOutput, calls=%fused_computation.7 | convolution fusion | flops 135331840 | bytes 1712640 | tf_op jit(solution)/shard_map/dot_general | solution.py:373
  3.8 1.8 %fusion.1 = f32[128,256]{1,0:T(8,128)S(1)} fusion(f32[128,256]{1,0:T(8,128)S(1)} %fusion.2, bf16[2048,256]{1,0:T(8,128)(2,1)} %param.19, bf16[128,2048]{1,0:T(8,128)(2,1)} %param.15, f32[2048]{0:T(1024)} %param.16, f32[128]{0:T(128)S(1)} %add_rsqrt_fusion.1), kind=kOutput, calls=%fused_computation.5 | convolution fusion | flops 135364608 | bytes 1843712 | tf_op jit(solution)/shard_map/dot_general | solution.py:374
  5.5 3.5 %collective-permute-start = (f32[2,256]{1,0:T(2,128)S(1)}, f32[2,256]{1,0:T(2,128)S(1)}, u32[]{:S(2)}, u32[]{:S(2)}) collective-permute-start(f32[2,256]{1,0:T(2,128)S(1)} %slice.25), channel_id=1, source_target_pairs={{0,4},{4,8},{8,12},{12,16},{16,20},{20,24},{24,28},{1,5},{5,9},{9,... | collective-permute-start | bytes 6152 | tf_op jit(solution)/shard_map/ppermute | solution.py:19
  9.0 0.0 copy-done.4
  9.0 0.0 copy-start.3
  9.0 0.0 copy-start.6
  9.0 0.0 copy-start.5
  9.0 77.1 %experts.1 = bf16[256,512]{1,0:T(8,128)(2,1)} custom-call(bf16[256,2048]{1,0:T(8,128)(2,1)} %x_ref.1, f32[1,2048]{1,0:T(1,128)} %bitcast.15, s32[2,256]{1,0:T(2,128)} %bitcast.16, f32[2,256]{1,0:T(2,128)} %bitcast.17, bf16[1,2048,896]{2,1,0:T(8,128)(2,1)} %gate_hbm.1, bf16[1,2048,896]{2,1,0:T(8,128)(2,1)} %up_hbm.1, bf16[1,3584,512]{2,1,0:T(8,128)(2,1)} %down_hbm.1), custom_call_target="tpu_custom_call" | custom-call | tf_op jit(solution)/shard_map/experts/pallas_call | solution.py:314
  86.2 0.0 copy-start.2
  86.2 0.0 copy-start.1
  86.2 0.0 collective-permute-done
  86.2 0.0 copy-done
  86.2 0.0 copy-done.3
  86.2 0.0 copy-done.6
  86.2 0.4 fusion.19
  86.6 0.1 copy.17
  86.8 0.1 copy.18
  86.9 0.0 copy-done.5
  86.9 5.8 %all_gather.3 = bf16[128,1024]{1,0:T(8,128)(2,1)S(1)} all-gather(bf16[128,256]{1,0:T(8,128)(2,1)S(1)} %multiply_convert_fusion), channel_id=1, replica_groups=mesh['ep'=8,'tp'=4] {'tp'}, dimensions={1}, use_global_device_ids=true | all-gather | bytes 327680 | tf_op jit(solution)/shard_map/all_gather | solution.py:392
  92.7 0.0 copy-done.2
  92.7 1.0 %convolution_convert_fusion = bf16[128,512]{1,0:T(8,128)(2,1)} fusion(bf16[128,1024]{1,0:T(8,128)(2,1)S(1)} %all_gather.3, bf16[1024,512]{1,0:T(8,128)(2,1)S(1)} %copy-done.2), kind=kOutput, calls=%fused_computation.2 | convolution fusion | flops 134283264 | bytes 1441792 | tf_op jit(solution)/shard_map/dot_general | solution.py:391
  93.6 0.0 copy-done.1
  93.6 0.7 copy.20
  (7 shorter events, 0.1 us)
Async XLA Ops:
  0.6 85.6 %copy-start = (bf16[2048,256]{1,0:T(8,128)(2,1)S(1)}, bf16[2048,256]{1,0:T(8,128)(2,1)}, u32[]{:S(2)}) copy-start(bf16[2048,256]{1,0:T(8,128)(2,1)} %param.17) | copy-start | bytes 3145732
  0.6 8.3 %copy-start.4 = (bf16[3,256]{1,0:T(4,128)(2,1)S(1)}, bf16[3,256]{1,0:T(4,128)(2,1)}, u32[]{:S(2)}) copy-start(bf16[3,256]{1,0:T(4,128)(2,1)} %param.20) | copy-start | bytes 4612
  5.5 80.7 %collective-permute-start = (f32[2,256]{1,0:T(2,128)S(1)}, f32[2,256]{1,0:T(2,128)S(1)}, u32[]{:S(2)}, u32[]{:S(2)}) collective-permute-start(f32[2,256]{1,0:T(2,128)S(1)} %slice.25), channel_id=1, source_target_pairs={{0,4},{4,8},{8,12},{12,16},{16,20},{20,24},{24,28},{1,5},{5,9},{9,... | collective-permute-start | bytes 6152 | tf_op jit(solution)/shard_map/ppermute | solution.py:19
  9.0 77.2 %copy-start.3 = (bf16[128,2048]{1,0:T(8,128)(2,1)S(1)}, bf16[128,2048]{1,0:T(8,128)(2,1)}, u32[]{:S(2)}) copy-start(bf16[128,2048]{1,0:T(8,128)(2,1)} %param.15) | copy-start | bytes 1572868
  9.0 77.2 %copy-start.6 = (f32[2048]{0:T(1024)S(1)}, f32[2048]{0:T(1024)}, u32[]{:S(2)}) copy-start(f32[2048]{0:T(1024)} %param.16) | copy-start | bytes 24580
  9.0 77.8 %copy-start.5 = (f32[256]{0:T(256)S(1)}, f32[256]{0:T(256)}, u32[]{:S(2)}) copy-start(f32[256]{0:T(256)} %param.21) | copy-start | bytes 3076
  86.2 6.5 %copy-start.2 = (bf16[1024,512]{1,0:T(8,128)(2,1)S(1)}, bf16[1024,512]{1,0:T(8,128)(2,1)}, u32[]{:S(2)}) copy-start(bf16[1024,512]{1,0:T(8,128)(2,1)} %param.22) | copy-start | bytes 3145732
  86.2 7.5 %copy-start.1 = (bf16[256,512]{1,0:T(8,128)(2,1)S(1)}, bf16[256,512]{1,0:T(8,128)(2,1)}, u32[]{:S(2)}) copy-start(bf16[256,512]{1,0:T(8,128)(2,1)} %experts.1) | copy-start | bytes 786436

commit v2 on v1

--- a/solution.py
+++ b/solution.py
@@ -45,13 +45,22 @@
 
 def experts_kernel(
     n_ep,
+    mix_ref,
+    mix_gain_ref,
+    kernel_ref,
+    group_gain_ref,
     x_ref,
     gain_ref,
     routes_ref,
     weight_ref,
+    outer_hbm,
+    inner_hbm,
+    value_hbm,
+    mix_out_hbm,
     gate_hbm,
     up_hbm,
     down_hbm,
+    mix_o_ref,
     o_ref,
     nb,
     xs,
@@ -63,6 +72,12 @@
     ret,
     whi,
     wlo,
+    na,
+    wmix,
+    wmo,
+    padded,
+    outer,
+    grouped,
     w_sem,
     s_sem,
     r_sem,
@@ -101,21 +116,32 @@
             )
         )
     fetch_down = pltpu.make_async_copy(down_hbm.at[0], wd, w_sem.at[2 * tiles])
+    fetch_mix = [
+        pltpu.make_async_copy(src, wmix.at[i], w_sem.at[2 * tiles + 1 + i])
+        for i, src in enumerate((outer_hbm, inner_hbm, value_hbm))
+    ]
+    fetch_mix_out = pltpu.make_async_copy(mix_out_hbm, wmo, w_sem.at[2 * tiles + 4])
     for a, b in fetches:
         a.start()
         b.start()
+    for copy in fetch_mix:
+        copy.start()
     fetch_down.start()
+    fetch_mix_out.start()
 
     step_rows = 32
 
-    def norm(i, carry):
-        at = pl.ds(pl.multiple_of(i * step_rows, step_rows), step_rows)
-        v = x_ref[at, :].astype(F32)
-        scale = lax.rsqrt(jnp.mean(v * v, axis=-1, keepdims=True) + EPS)
-        nb[at, :] = (v * scale * gain_ref[...]).astype(BF16)
-        return carry
-
-    lax.fori_loop(0, rows // step_rows, norm, 0)
+    def normalize(src, gain, dst):
+        def norm(i, carry):
+            at = pl.ds(pl.multiple_of(i * step_rows, step_rows), step_rows)
+            v = src[at, :].astype(F32)
+            scale = lax.rsqrt(jnp.mean(v * v, axis=-1, keepdims=True) + EPS)
+            dst[at, :] = (v * scale * gain[...]).astype(BF16)
+            return carry
+
+        lax.fori_loop(0, src.shape[0] // step_rows, norm, 0)
+
+    normalize(x_ref, gain_ref, nb)
 
     first = routes_ref[0:1, :]
     second = routes_ref[1:2, :]
@@ -244,7 +270,60 @@
         if m >= half:
             relay[m].wait_recv()
 
+    mix_rows, channels = outer.shape
+    halo = padded.shape[0] - mix_rows
+    ahead = {"ep": lax.rem(ep + 1, n_ep)}
+    send_halo = remote(padded.at[pl.ds(mix_rows, halo)], padded.at[pl.ds(0, halo)], 8, 0, ahead)
+    mix_partner = remote(grouped.at[tp], grouped.at[tp], 8, 1, partner)
+    mix_across = remote(grouped.at[tp], grouped.at[tp], 8, 2, across)
+    mix_relay = remote(grouped.at[over_tp], grouped.at[over_tp], 8, 3, partner)
+
+    def mix_project():
+        normalize(mix_ref, mix_gain_ref, na)
+        for copy in fetch_mix:
+            copy.wait()
+        outer[...] = matmul(na[...], wmix[0]).astype(BF16)
+        inner = matmul(na[...], wmix[1]).astype(BF16).astype(F32)
+        padded[pl.ds(halo, mix_rows), :] = inner * matmul(na[...], wmix[2]).astype(BF16).astype(F32)
+        send_halo.start()
+
+    def mix_convolve():
+        send_halo.wait_recv()
+        taps = kernel_ref[...].astype(F32)
+        row = lax.broadcasted_iota(jnp.int32, (mix_rows, channels), 0)
+        row = row + jnp.where(ep == 0, 0, mix_rows)
+        conv = taps[2:3, :] * padded[pl.ds(halo, mix_rows), :]
+        for back_by in (1, 2):
+            shifted = padded[pl.ds(halo - back_by, mix_rows), :]
+            conv = conv + taps[2 - back_by : 3 - back_by, :] * jnp.where(
+                row >= back_by, shifted, 0.0
+            )
+        gated = outer[...].astype(F32) * conv
+        squares = gated * gated
+        group = lax.broadcasted_iota(jnp.int32, (mix_rows, channels), 1) // GROUP
+        scale = jnp.zeros_like(gated)
+        for i in range(channels // GROUP):
+            mean = jnp.sum(jnp.where(group == i, squares, 0.0), axis=-1, keepdims=True) / GROUP
+            scale = jnp.where(group == i, lax.rsqrt(mean + EPS), scale)
+        grouped[tp] = (gated * scale * group_gain_ref[...]).astype(BF16)
+        mix_across.start()
+        mix_partner.start()
+
+    def mix_pass():
+        mix_across.wait_recv()
+        mix_relay.start()
+
+    def mix_contract():
+        fetch_mix_out.wait()
+        mix_partner.wait_recv()
+        mix_relay.wait_recv()
+        acc = matmul(grouped[0], wmo[0:channels, :])
+        for k in range(1, grouped.shape[0]):
+            acc = acc + matmul(grouped[k], wmo[k * channels : (k + 1) * channels, :])
+        mix_o_ref[...] = acc.astype(BF16)
+
     expand(0)
+    mix_project()
     for m in range(n_ep):
         picked = jnp.where(first == flip(ep, m, n_ep), weight_ref[0:1, :], weight_ref[1:2, :])
         scaled = (place[m] * picked).T
@@ -256,6 +335,7 @@
         ready(m)
         expand(m)
         if m == 1:
+            mix_convolve()
             fetch_down.wait()
         if m >= 2:
             pass_hidden(m - 2)
@@ -265,7 +345,10 @@
         if m == half:
             pass_hidden(half - 2)
             contract(half - 2)
+        if m == half:
+            mix_pass()
     pass_hidden(half - 1)
+    mix_contract()
     for m in range(half, n_ep):
         pass_relay(m)
         ready(m)
@@ -289,6 +372,8 @@
         total = high + low if total is None else total + (high + low)
     o_ref[...] = total.astype(BF16)
 
+    for copy in (send_halo, mix_partner, mix_across, mix_relay):
+        copy.wait_send()
     for m in range(n_ep):
         for copy in (hid_partner[m], hid_across[m], hid_relay[m], from_source[m], back[m]):
             if copy is not None:
@@ -298,24 +383,44 @@
                 table[m].wait_send()
 
 
-def experts_fused(
-    expert_input, expert_gain, routes, route_weight, expert_gate, expert_up, expert_down
+def fused(
+    mixer_input,
+    mixer_gain,
+    outer_weight,
+    inner_weight,
+    value_weight,
+    conv_kernel,
+    group_gain,
+    mixer_out_weight,
+    expert_input,
+    expert_gain,
+    routes,
+    route_weight,
+    expert_gate,
+    expert_up,
+    expert_down,
 ):
     n_ep, n_tp = lax.axis_size("ep"), lax.axis_size("tp")
     rows, width = expert_input.shape
+    mix_rows = mixer_input.shape[0]
+    channels = outer_weight.shape[1]
     cap = 2 * routes.shape[1] * rows // n_ep
     span = width // n_tp
     part = expert_gate.shape[2]
     tile = 128
     tiles = part // tile
     full, out_cols = expert_down.shape[1:]
+    mix_cols = mixer_out_weight.shape[1]
     vmem = pl.BlockSpec(memory_space=pltpu.VMEM)
     hbm = pl.BlockSpec(memory_space=pl.ANY)
     return pl.pallas_call(
         functools.partial(experts_kernel, n_ep),
-        out_shape=jax.ShapeDtypeStruct((rows, out_cols), BF16),
-        in_specs=[vmem] * 4 + [hbm] * 3,
-        out_specs=vmem,
+        out_shape=(
+            jax.ShapeDtypeStruct((mix_rows, mix_cols), BF16),
+            jax.ShapeDtypeStruct((rows, out_cols), BF16),
+        ),
+        in_specs=[vmem] * 8 + [hbm] * 7,
+        out_specs=(vmem, vmem),
         scratch_shapes=[
             pltpu.VMEM((rows, width), BF16),
             pltpu.VMEM((n_ep, 2, cap, span), BF16),
@@ -327,19 +432,33 @@
             pltpu.VMEM((n_ep, cap, out_cols), BF16),
             pltpu.VMEM((rows, n_ep * cap), BF16),
             pltpu.VMEM((rows, n_ep * cap), BF16),
-            pltpu.SemaphoreType.DMA((2 * tiles + 1,)),
-            pltpu.SemaphoreType.DMA((8, n_ep)),
-            pltpu.SemaphoreType.DMA((8, n_ep)),
+            pltpu.VMEM((mix_rows, width), BF16),
+            pltpu.VMEM((3, width, channels), BF16),
+            pltpu.VMEM((channels * n_tp, mix_cols), BF16),
+            pltpu.VMEM((8 + mix_rows, channels), F32),
+            pltpu.VMEM((mix_rows, channels), BF16),
+            pltpu.VMEM((n_tp, mix_rows, channels), BF16),
+            pltpu.SemaphoreType.DMA((2 * tiles + 5,)),
+            pltpu.SemaphoreType.DMA((9, n_ep)),
+            pltpu.SemaphoreType.DMA((9, n_ep)),
         ],
         compiler_params=pltpu.CompilerParams(
-            collective_id=0, has_side_effects=True, vmem_limit_bytes=56 * 1024 * 1024
+            collective_id=0, has_side_effects=True, vmem_limit_bytes=60 * 1024 * 1024
         ),
-        name="experts",
+        name="layer",
     )(
+        mixer_input,
+        mixer_gain.reshape(1, -1),
+        conv_kernel,
+        group_gain.reshape(1, -1),
         expert_input,
         expert_gain.reshape(1, -1),
         routes.T,
         route_weight.T,
+        outer_weight,
+        inner_weight,
+        value_weight,
+        mixer_out_weight,
         expert_gate,
         expert_up,
         expert_down,
@@ -455,11 +574,10 @@
 
 
 def per_device(*args):
-    mixed = mixer_xla(*args[:8])
     n_ep, n_tp = lax.axis_size("ep"), lax.axis_size("tp")
     if fits(n_ep, n_tp, args[10], args[12]):
-        return mixed, experts_fused(*args[8:])
-    return mixed, experts_xla(*args[8:])
+        return fused(*args)
+    return mixer_xla(*args[:8]), experts_xla(*args[8:])
 
 
 def solution(mesh):

time: 95.9 us -> 96 us (level); the launches traced: 94.4 us -> 95.8 us
  Pallas kernels: 77.1 us -> 91.9 us
  blocking collectives: 5.78 us -> 0 us
  matrix products: 4.84 us -> 0 us
  starting transfers between devices: 3.45 us -> 0 us
  local copies, waits for them, and re-layouts: 0.95 us -> 3.24 us
  other arithmetic: 1.38 us -> 0 us
    pallas_call x1, Pallas kernels: 77.1 us -> 91.9 us  [fused(): pl.pallas_call(functools.partial(experts_kernel, n_ep), out_shape=(jax.Sh...]
    all_gather x1 -> x0, blocking collectives: 5.78 us -> none  [mixer_xla(): lax.all_gather(grouped, 'tp', axis=1, tiled=True)]
    dot_general x4 -> x0, matrix products: 4.84 us -> none  [the longest x1 1.76 us: mixer_xla(): jnp.dot(normed_a, inner_weight, preferred_element_type=jnp.float32)]
    ppermute x1 -> x0, starting transfers between devices: 3.45 us -> none  [from_behind(): return lax.ppermute(block, axis, route)]
    unnamed x15 -> x2, local copies, waits for them, and re-layouts: 0.75 us -> 3.24 us
    reduce_sum x2 -> x0, other arithmetic: 1.35 us -> none  [rms_scale(): scale = lax.rsqrt(jnp.mean(floats * floats, axis=-1, keepdims=True) + EPS)]
  transfers between devices with their start and end apart: 1 -> 0, of which waited for: 0 -> 0; matrix products, arithmetic and copies ran while one was open for 0% -> 0% of each run, Pallas kernels for 82% -> 0%
where the time goes in v2:
time: 96 us; the launch traced here: 95.8 us
  Pallas kernels  91.9 us (96%)
  local copies, waits for them, and re-layouts  3.24 us (3%)
    pallas_call x1, Pallas kernels, fused(): pl.pallas_call(functools.partial(experts_kernel, n_ep), out_shape=(jax.Sh...  91.9 us
    unnamed x2, local copies, waits for them, and re-layouts  3.24 us

profile of v2, /device:TPU:18, one launch (start us, length us, event | category | flops | bytes accessed | tf_op | source)
XLA Modules:
  0.0 95.8 jit_solution(15374653882910264536)
XLA Ops:
  0.6 91.9 %layer.1 = (bf16[128,512]{1,0:T(8,128)(2,1)}, bf16[256,512]{1,0:T(8,128)(2,1)}) custom-call(bf16[128,2048]{1,0:T(8,128)(2,1)} %mix_ref.1, f32[1,2048]{1,0:T(1,128)} %bitcast.5, bf16[3,256]{1,0:T(4,128)(2,1)} %kernel_ref.1, f32[1,256]{1,0:T(1,128)} %bitcast.9, bf16[256,2048]{1,0:T(8,128)(2,1)} %x_ref.1, f32[1,2048]{1,0:T(1,128)} %bitcast.6, ...), custom_call_target="tpu_custom_call" | custom-call | tf_op jit(solution)/shard_map/layer/pallas_call | solution.py:416
  92.5 1.6 %copy.19 = bf16[128,512]{1,0:T(8,128)(2,1)} copy(bf16[128,512]{1,0:T(8,128)(2,1)} %get-tuple-element.4) | data formatting | bytes 262144
  94.1 1.7 %copy.20 = bf16[256,512]{1,0:T(8,128)(2,1)} copy(bf16[256,512]{1,0:T(8,128)(2,1)} %get-tuple-element.5) | data formatting | bytes 524288

commit v3 on v2

--- a/solution.py
+++ b/solution.py
@@ -41,6 +41,25 @@
 
 def matmul(a, b):
     return jnp.dot(a, b, preferred_element_type=F32)
+
+
+def send_order(n_ep):
+    half = n_ep // 2
+    return [1, *range(half, n_ep), *range(2, half)]
+
+
+def schedule(n_ep):
+    half = n_ep // 2
+    early = [*range(half, half + half // 2)]
+    late = [*range(half + half // 2, n_ep)]
+    steps = [("pass_far", m) for m in early]
+    steps += [("finish", 0), ("mix", 0)]
+    steps += [("far", m) for m in early] + [("pass_far", m) for m in late] + [("finish", 1)]
+    done = list(early)
+    for m, other in zip(range(2, half), late):
+        steps += [("near", m), ("finish", done.pop(0)), ("far", other), ("finish", done.pop(0))]
+        done += [m, other]
+    return steps + [("finish", m) for m in done]
 
 
 def experts_kernel(
@@ -192,7 +211,7 @@
         if m:
             back[m] = remote(rs.at[m], ret.at[m], 7, m, {"ep": flip(ep, m, n_ep)})
 
-    for m in range(1, n_ep):
+    for m in send_order(n_ep):
         chosen = place[m].astype(BF16)
         if m < half:
             for k in range(2):
@@ -201,7 +220,7 @@
         else:
             at = pl.ds(pl.multiple_of(tp * span, span), span)
             xs[m, 0] = matmul(chosen, nb[:, at]).astype(BF16)
-        if m == 1:
+        if m == send_order(n_ep)[0]:
             pl.semaphore_wait(barrier, len(peers))
         from_source[m].start()
     chosen = place[0].astype(BF16)
@@ -322,46 +341,44 @@
             acc = acc + matmul(grouped[k], wmo[k * channels : (k + 1) * channels, :])
         mix_o_ref[...] = acc.astype(BF16)
 
-    expand(0)
-    mix_project()
-    for m in range(n_ep):
-        picked = jnp.where(first == flip(ep, m, n_ep), weight_ref[0:1, :], weight_ref[1:2, :])
-        scaled = (place[m] * picked).T
-        high = scaled.astype(BF16)
-        whi[:, m * cap : (m + 1) * cap] = high
-        wlo[:, m * cap : (m + 1) * cap] = (scaled - high.astype(F32)).astype(BF16)
-    for m in range(1, half):
+    def build_weights():
+        for m in range(n_ep):
+            picked = jnp.where(first == flip(ep, m, n_ep), weight_ref[0:1, :], weight_ref[1:2, :])
+            scaled = (place[m] * picked).T
+            high = scaled.astype(BF16)
+            whi[:, m * cap : (m + 1) * cap] = high
+            wlo[:, m * cap : (m + 1) * cap] = (scaled - high.astype(F32)).astype(BF16)
+
+    def near(m):
         pass_near(m)
         ready(m)
         expand(m)
-        if m == 1:
-            mix_convolve()
-            fetch_down.wait()
-        if m >= 2:
-            pass_hidden(m - 2)
-            contract(m - 2)
-    for m in range(half, n_ep):
-        pass_far(m)
-        if m == half:
-            pass_hidden(half - 2)
-            contract(half - 2)
-        if m == half:
-            mix_pass()
-    pass_hidden(half - 1)
-    mix_contract()
-    for m in range(half, n_ep):
+
+    def far(m):
         pass_relay(m)
         ready(m)
         expand(m)
-        if m == half:
-            contract(half - 1)
-        if m - 2 >= half:
-            pass_hidden(m - 2)
-            contract(m - 2)
-    pass_hidden(n_ep - 2)
-    contract(n_ep - 2)
-    pass_hidden(n_ep - 1)
-    contract(n_ep - 1)
+
+    def finish(m):
+        pass_hidden(m)
+        contract(m)
+
+    steps = dict(
+        near=near, far=far, finish=finish, pass_far=pass_far, pass_hidden=pass_hidden,
+        contract=contract,
+    )
+    expand(0)
+    mix_project()
+    build_weights()
+    near(1)
+    mix_convolve()
+    fetch_down.wait()
+    for step, m in schedule(n_ep):
+        if step == "mix":
+            mix_pass()
+            mix_contract()
+        else:
+            steps[step](m)
 
     total = None
     for m in range(n_ep):

time: 96 us -> 94.6 us (0.985)
  Pallas kernels: 91.9 us -> 90.2 us
    pallas_call x1, Pallas kernels: 91.9 us -> 90.2 us  [fused(): pl.pallas_call(functools.partial(experts_kernel, n_ep), out_shape=(jax.Sh...]
where the time goes in v3:
time: 94.6 us; the launch traced here: 94.1 us
  Pallas kernels  90.2 us (95%)
  local copies, waits for them, and re-layouts  3.24 us (3%)
    pallas_call x1, Pallas kernels, fused(): pl.pallas_call(functools.partial(experts_kernel, n_ep), out_shape=(jax.Sh...  90.2 us
    unnamed x2, local copies, waits for them, and re-layouts  3.24 us

profile of v3, /device:TPU:18, one launch (start us, length us, event | category | flops | bytes accessed | tf_op | source)
XLA Modules:
  0.0 94.1 jit_solution(14722387767765875128)
XLA Ops:
  0.6 90.2 %layer.1 = (bf16[128,512]{1,0:T(8,128)(2,1)}, bf16[256,512]{1,0:T(8,128)(2,1)}) custom-call(bf16[128,2048]{1,0:T(8,128)(2,1)} %mix_ref.1, f32[1,2048]{1,0:T(1,128)} %bitcast.5, bf16[3,256]{1,0:T(4,128)(2,1)} %kernel_ref.1, f32[1,256]{1,0:T(1,128)} %bitcast.9, bf16[256,2048]{1,0:T(8,128)(2,1)} %x_ref.1, f32[1,2048]{1,0:T(1,128)} %bitcast.6, ...), custom_call_target="tpu_custom_call" | custom-call | tf_op jit(solution)/shard_map/layer/pallas_call | solution.py:433
  90.9 1.6 %copy.19 = bf16[128,512]{1,0:T(8,128)(2,1)} copy(bf16[128,512]{1,0:T(8,128)(2,1)} %get-tuple-element.4) | data formatting | bytes 262144
  92.5 1.7 %copy.20 = bf16[256,512]{1,0:T(8,128)(2,1)} copy(bf16[256,512]{1,0:T(8,128)(2,1)} %get-tuple-element.5) | data formatting | bytes 524288
